TPU v7x, 32 devices: a whole 2x2x4 slice. The times are simulated.
32 devices in a mesh: gr: 2 (over x), sp: 8 (over z, y), tp: 2 (over core).
Axes of the slice: x: 2, y: 2, z: 4, core: 2. Of those that a mesh axis runs over, the one named last changes fastest.
Arguments:
- tokens: bfloat16 [4, 2, 2048, 4096], P('gr', 'tp', 'sp'), may hold values from -6 to 6
- ln_gain: bfloat16 [4096], replicated, may hold values from 0.099609375 to 1.8984375
- w_key: bfloat16 [4096, 256], P('sp'), may hold values from -0.09375 to 0.09375
- w_value: bfloat16 [4096, 256], P('sp'), may hold values from -0.09375 to 0.09375
- queries: bfloat16 [16, 512], P(('gr', 'sp')), may hold values from -6 to 6
- head_shift: float32 [4, 8], replicated
- key_shift: float32 [16, 4096], P(('gr', 'sp'), 'tp')
Outputs:
- kv_cache: bfloat16 [16, 4096, 128], P(('gr', 'sp'), 'tp')
- first_read: float32 [16, 512], P(('gr', 'sp'))
All inputs are finite; a program needn't handle non-finite values.
Results may differ from a plain program's by a relative error of at most 0.0064.
Values may be sent and summed in bfloat16 or wider, within the bound.
A program may use at most 64 MiB of HBM per device.

v0:
```python
import functools

import jax
import jax.numpy as jnp
from jax import lax
from jax.experimental import pallas as pl
from jax.experimental.pallas import tpu as pltpu
from jax.sharding import PartitionSpec as P

epsilon = 1e-05
STAGES = 4
NORM_AT = (0.5, 2.6, 3.1, 5.1)
LAG, LANE, HOP, CROSS = 3.0, 1.0, 2.5, 1.0
ORDERS = ((0, 0, 0, 0), (1, 1, 1, 1))
MESH = pl.DeviceIdType.MESH


def layout(mesh):
    sp, gr, tp = mesh.shape["sp"], mesh.shape["gr"], mesh.shape["tp"]
    inner = 1
    while inner * inner * 4 <= sp and sp % (inner * 2) == 0:
        inner *= 2
    return sp // inner, inner, gr, tp


def body(
    grid, head_size,
    tokens, gain, w_key, w_value, queries, head_shift, key_shift,
    cache, read,
    raw, normed, weights, acc, outgoing, incoming, totals, parts,
    send_sem, recv_sem, load_sem,
):
    depth, inner, groups, sections = grid
    seats = depth * inner
    seat, group, section = lax.axis_index("sp"), lax.axis_index("gr"), lax.axis_index("tp")
    lane, place = seat // inner, seat % inner
    rows, width = raw.shape
    shard, columns = w_key.shape
    piece = shard // (groups * sections)
    kv_heads, heads = head_shift.shape
    seqs = seats // kv_heads
    sub = rows // seqs
    half = sub // 2
    stage_rows = rows // STAGES

    sent = []

    def push(source, target, **where):
        at = len(sent)
        copy = pltpu.make_async_remote_copy(
            src_ref=source, dst_ref=target, send_sem=send_sem.at[at], recv_sem=recv_sem.at[at],
            device_id=where, device_id_type=MESH,
        )
        copy.start()
        sent.append(copy)
        return copy

    own = pl.ds(pl.multiple_of(seat * shard, shard), shard)
    loads = []
    for at, source in enumerate((w_key, w_value)):
        loads.append(pltpu.make_async_copy(source, weights.at[at, own], load_sem.at[at]))
        loads[-1].start()
    fills = []
    for at in range(STAGES):
        block = pl.ds(at * stage_rows, stage_rows)
        fills.append(pltpu.make_async_copy(tokens.at[block], raw.at[block], load_sem.at[2 + at]))
        fills[-1].start()

    def seat_at(k, j):
        return lax.rem(lane + depth - k, depth) * inner + lax.rem(place + inner - j, inner)

    barrier = pltpu.get_barrier_semaphore()
    for i in range(1, seats):
        pl.semaphore_signal(barrier, 1, device_id={"sp": lax.rem(seat + i, seats)}, device_id_type=MESH)
    for i in range(1, groups):
        pl.semaphore_signal(barrier, 1, device_id={"gr": lax.rem(group + i, groups)}, device_id_type=MESH)
    for i in range(1, sections):
        pl.semaphore_signal(barrier, 1, device_id={"tp": lax.rem(section + i, sections)}, device_id_type=MESH)
    pl.semaphore_wait(barrier, seats + groups + sections - 3)

    def block_of(m, k, j, g):
        share = lax.rem(group + groups - g, groups) * sections + section
        start = seat_at(k, j) * shard + share * piece
        return weights.at[m, pl.ds(pl.multiple_of(start, piece), piece)]

    got = {}
    crossed = {}

    def along_lane(m):
        for k in range(1, depth):
            to = lax.rem(lane + k, depth) * inner + place
            block = block_of(m, 0, 0, 0)
            got[m, k, 0, 0] = push(block, block, sp=to)

    def along_place(m, k, g):
        for j in range(1, inner):
            to = lane * inner + lax.rem(place + j, inner)
            block = block_of(m, k, 0, g)
            got[m, k, j, g] = push(block, block, sp=to)

    def along_group(m, k, j):
        if k == 0 and j == 0:
            return
        for g in range(1, groups):
            block = block_of(m, k, j, 0)
            got[m, k, j, g] = push(block, block, gr=lax.rem(group + g, groups))

    def along_section(m, k, j, g):
        if k == 0 and j == 0:
            return
        block = block_of(m, k, j, g)
        for t in range(1, sections):
            copy = push(block, block, tp=lax.rem(section + t, sections))
            crossed.setdefault((m, k), []).append(copy)

    def first(m, k):
        if k > 0:
            got[m, k, 0, 0].wait_recv()
        if ORDERS[m][k % len(ORDERS[m])]:
            along_group(m, k, 0)
            along_place(m, k, 0)
        else:
            along_place(m, k, 0)
            along_group(m, k, 0)
        along_section(m, k, 0, 0)
        if ORDERS[m][k % len(ORDERS[m])] and k == 0:
            second(m, k)

    def second(m, k):
        if ORDERS[m][k % len(ORDERS[m])]:
            for g in range(1, groups):
                if k > 0:
                    got[m, k, 0, g].wait_recv()
                along_place(m, k, g)
                along_section(m, k, 0, g)
        else:
            for j in range(1, inner):
                got[m, k, j, 0].wait_recv()
                along_group(m, k, j)
                along_section(m, k, j, 0)

    def third(m, k):
        if ORDERS[m][k % len(ORDERS[m])]:
            lasts = [(j, g) for j in range(1, inner) for g in range(groups)]
        else:
            lasts = [(j, g) for j in range(inner) for g in range(1, groups) if k > 0 or j > 0]
        for j, g in lasts:
            got[m, k, j, g].wait_recv()
            along_section(m, k, j, g)

    def normalise(at):
        fills[at].wait()
        step = 32

        @pl.loop(0, stage_rows // step)
        def _(i):
            here = pl.ds(pl.multiple_of(at * stage_rows + i * step, step), step)
            x = raw[here, :].astype(jnp.float32)
            mean = jnp.mean(x, axis=1, keepdims=True)
            centred = x - mean
            var = jnp.mean(centred * centred, axis=1, keepdims=True)
            scale = gain[...].astype(jnp.float32).reshape(1, width)
            normed[here, :] = (centred * lax.rsqrt(var + epsilon) * scale).astype(jnp.bfloat16)

    def multiply(m, k):
        for copy in crossed.get((m, k), ()):
            copy.wait_recv()
        span = inner * shard
        start = pl.multiple_of(lax.rem(lane + depth - k, depth) * span, span)
        out = jnp.dot(normed[:, pl.ds(start, span)], weights[m, pl.ds(start, span), :], preferred_element_type=jnp.float32)
        if k == 0:
            acc[m] = out
        else:
            acc[m] += out

    swapped = {}

    def exchange(m):
        for pair in range(seats):
            seq, head = pair // kv_heads, pair % kv_heads
            cut = slice(head * head_size, (head + 1) * head_size)
            first = acc[m, seq * sub:seq * sub + half, cut]
            second = acc[m, seq * sub + half:(seq + 1) * sub, cut]
            outgoing[m, pair] = jnp.concatenate([first, second], axis=1).astype(jnp.bfloat16)
        for i in range(1, seats):
            to = lax.rem(seat + i, seats)
            swapped[m, i] = push(outgoing.at[m, to], incoming.at[m, seat], sp=to)
        incoming[m, pl.ds(seat, 1)] = outgoing[m, pl.ds(seat, 1)]

    loads[0].wait()
    first(0, 0)
    along_lane(0)
    loads[1].wait()
    along_lane(1)
    first(1, 0)
    steps = [(NORM_AT[at], "norm", normalise, (at,)) for at in range(STAGES)]
    for m in range(2):
        end = 0.0
        for k in range(depth):
            base = m * LAG + k * LANE
            if k > 0:
                steps.append((base, "first", first, (m, k)))
            if not (k == 0 and ORDERS[m][0]):
                steps.append((base + HOP, "second", second, (m, k)))
            steps.append((base + 2 * HOP, "third", third, (m, k)))
            end = max(end, base + 2 * HOP + CROSS, NORM_AT[-1] + 0.01 * (k + 1))
            steps.append((end, "times", multiply, (m, k)))
        steps.append((end + 0.001, "trade", exchange, (m,)))
    for _, _, call, arguments in sorted(steps, key=lambda step: step[0]):
        call(*arguments)

    query = queries[...].astype(jnp.float32)
    query = jnp.concatenate([query[:, g * head_size:(g + 1) * head_size] for g in range(heads)], axis=0)
    blank = jnp.zeros_like(query)
    query = jnp.concatenate(
        [jnp.concatenate([query, blank], axis=1), jnp.concatenate([blank, query], axis=1)], axis=0
    ).astype(jnp.bfloat16)
    mine = lax.broadcasted_iota(jnp.int32, (kv_heads, heads), 0) == lax.rem(seat, kv_heads)
    shift = jnp.sum(jnp.where(mine, head_shift[...], 0.0), axis=0, keepdims=True)
    eye = lax.broadcasted_iota(jnp.int32, (heads, heads), 0) == lax.broadcasted_iota(jnp.int32, (heads, heads), 1)
    shift = jnp.sum(jnp.where(eye, jnp.broadcast_to(shift, (heads, heads)), 0.0), axis=1, keepdims=True)
    later = (
        lax.broadcasted_iota(jnp.int32, (half, half), 0) > lax.broadcasted_iota(jnp.int32, (half, half), 1)
    ).astype(jnp.float32)

    for i in range(1, seats):
        swapped[0, i].wait_recv()
    keys = incoming[0].reshape(seats * half, 2 * head_size)
    logits = lax.dot_general(query, keys, (((1,), (1,)), ((), ())), preferred_element_type=jnp.float32)
    logits = logits * head_size ** (-0.5)
    betas, keeps = [], []
    for at in range(2 * seats):
        q, h = at // 2, at % 2
        z = logits[h * heads:(h + 1) * heads, q * half:(q + 1) * half]
        z = z + shift + key_shift[:, at * half:(at + 1) * half]
        tail = jnp.log1p(jnp.exp(-jnp.abs(z)))
        betas.append(jnp.minimum(z, 0.0) - tail)
        keeps.append(jnp.minimum(-z, 0.0) - tail)
    within = jnp.dot(
        jnp.concatenate(keeps, axis=0), later, preferred_element_type=jnp.float32, precision=lax.Precision.HIGHEST
    )
    running = jnp.zeros((heads, 1), jnp.float32)
    local = [None] * (2 * seats)
    for at in reversed(range(2 * seats)):
        local[at] = jnp.exp(betas[at] + within[at * heads:(at + 1) * heads] + running)
        running = running + jnp.sum(keeps[at], axis=1, keepdims=True)
    local = jnp.concatenate(
        [jnp.concatenate(local[0::2], axis=1), jnp.concatenate(local[1::2], axis=1)], axis=0
    ).astype(jnp.bfloat16)
    totals[section] = jnp.broadcast_to(running, totals.shape[1:])
    arrivals = [
        push(totals.at[section], totals.at[section], tp=lax.rem(section + t, sections)) for t in range(1, sections)
    ]
    for copy in arrivals:
        copy.wait_recv()
    carry = jnp.zeros((heads, head_size), jnp.float32)
    for t in reversed(range(sections)):
        carry = carry + jnp.where(section < t, totals[t][:, :head_size], 0.0)
    carry = jnp.exp(carry)

    for i in range(1, seats):
        swapped[1, i].wait_recv()
    values = incoming[1].reshape(seats * half, 2 * head_size)
    part = jnp.dot(local, values, preferred_element_type=jnp.float32)
    part = carry * (part[:heads, :head_size] + part[heads:, head_size:])
    parts[section] = jnp.concatenate([part, part], axis=1)
    arrivals = [
        push(parts.at[section], parts.at[section], tp=lax.rem(section + t, sections)) for t in range(1, sections)
    ]
    for q in range(seats):
        for h in range(2):
            cut = slice(h * head_size, (h + 1) * head_size)
            start = (2 * q + h) * half
            cache[0, start:start + half, :] = jnp.concatenate([incoming[0, q][:, cut], incoming[1, q][:, cut]], axis=1)
    for copy in arrivals:
        copy.wait_recv()
    total = parts[0]
    for t in range(1, sections):
        total = total + parts[t]
    for g in range(heads):
        read[:, g * head_size:(g + 1) * head_size] = total[g:g + 1, :head_size]
    for copy in sent:
        copy.wait_send()


def hand_over(cache, read, cache_out, read_out):
    cache_out[...] = cache[...]
    read_out[...] = read[...]


def copies(grid):
    depth, inner, groups, sections = grid
    pieces = depth * inner * groups
    gather = pieces + (pieces - groups) * (sections - 1)
    return 2 * gather + 2 * (depth * inner - 1) + 2 * (sections - 1)


def local(grid, tokens, ln_gain, w_key, w_value, queries, head_shift, key_shift):
    depth, inner, groups, sections = grid
    seats = depth * inner
    seqs, _, sub, width = tokens.shape
    rows = seqs * sub
    columns = w_key.shape[1]
    kv_heads, heads = head_shift.shape
    head_size = columns // kv_heads
    vmem = pl.BlockSpec(memory_space=pltpu.VMEM)
    hbm = pl.BlockSpec(memory_space=pl.ANY)
    count = copies(grid)
    cache, read = pl.pallas_call(
        functools.partial(body, grid, head_size),
        out_shape=(
            jax.ShapeDtypeStruct((1, seats * sub, 2 * head_size), jnp.bfloat16),
            jax.ShapeDtypeStruct((1, heads * head_size), jnp.float32),
        ),
        in_specs=[hbm, vmem, hbm, hbm, vmem, vmem, vmem],
        out_specs=(vmem, vmem),
        scratch_shapes=[
            pltpu.VMEM((rows, width), jnp.bfloat16),
            pltpu.VMEM((rows, width), jnp.bfloat16),
            pltpu.VMEM((2, width, columns), jnp.bfloat16),
            pltpu.VMEM((2, rows, columns), jnp.float32),
            pltpu.VMEM((2, seats, sub // 2, 2 * head_size), jnp.bfloat16),
            pltpu.VMEM((2, seats, sub // 2, 2 * head_size), jnp.bfloat16),
            pltpu.VMEM((sections, heads, 2 * head_size), jnp.float32),
            pltpu.VMEM((sections, heads, 2 * head_size), jnp.float32),
            pltpu.SemaphoreType.DMA((count,)),
            pltpu.SemaphoreType.DMA((count,)),
            pltpu.SemaphoreType.DMA((2 + STAGES,)),
        ],
        compiler_params=pltpu.CompilerParams(
            collective_id=0, has_side_effects=True, vmem_limit_bytes=60 * 1024 * 1024
        ),
    )(tokens.reshape(rows, width), ln_gain, w_key, w_value, queries, head_shift, key_shift)
    return pl.pallas_call(
        hand_over,
        out_shape=(jax.ShapeDtypeStruct(cache.shape, cache.dtype), jax.ShapeDtypeStruct(read.shape, read.dtype)),
        in_specs=[vmem, vmem],
        out_specs=(vmem, vmem),
    )(cache, read)


def solution(mesh):
    in_specs = (
        P("gr", "tp", "sp", None),
        P(),
        P("sp", None),
        P("sp", None),
        P(("gr", "sp"), None),
        P(),
        P(("gr", "sp"), "tp"),
    )
    out_specs = (P(("gr", "sp"), "tp", None), P(("gr", "sp"), None))
    return jax.shard_map(
        functools.partial(local, layout(mesh)), mesh=mesh, in_specs=in_specs, out_specs=out_specs, check_vma=False
    )
```

profile of v0, /device:TPU:13, one launch (start us, length us, event | category | flops | bytes accessed | tf_op | source)
XLA Modules:
  0.0 46.4 jit_solution(15329165219051864417)
XLA Ops:
  0.6 43.9 %shard_map.86 = (bf16[1,2048,128]{2,1,0:T(8,128)(2,1)}, f32[1,512]{1,0:T(1,128)}) custom-call(bf16[512,4096]{1,0:T(8,128)(2,1)} %bitcast.1, bf16[4096]{0:T(1024)(128)(2,1)} %gain.1, bf16[512,256]{1,0:T(8,128)(2,1)} %w_key.1, bf16[512,256]{1,0:T(8,128)(2,1)} %w_value.1, bf16[1,512]{1,0:T(2,128)(2,1)} %queries.1, f32[4,8]{1,0:T(4,128)} %head_shift.1, ...), custom_call_target="tpu_custom_call" | custom-call | tf_op jit(solution)/shard_map/pallas_call | solution.py:309
  44.6 1.9 %shard_map.87 = (bf16[1,2048,128]{2,1,0:T(8,128)(2,1)}, f32[1,512]{1,0:T(1,128)}) custom-call(bf16[1,2048,128]{2,1,0:T(8,128)(2,1)} %get-tuple-element.4.cache, f32[1,512]{1,0:T(1,128)} %get-tuple-element.5.read), custom_call_target="tpu_custom_call" | custom-call | tf_op jit(solution)/shard_map/pallas_call | solution.py:334
where the time goes:
time: 46.9 us; the launch traced here: 46.4 us
  Pallas kernels  45.8 us (98%)
  between operations  0.64 us (1%)
    pallas_call x1, Pallas kernels, local(): pl.pallas_call(functools.partial(body, grid, head_size), out_shape=(jax.S...  43.9 us
    pallas_call x1, Pallas kernels, local(): pl.pallas_call(hand_over, out_shape=(jax.ShapeDtypeStruct(cache.shape, ca...  1.87 us

commit v1 on v0

v1 whole, which is shorter than its diff:
```python
import functools

import jax
import jax.numpy as jnp
from jax import lax
from jax.experimental import pallas as pl
from jax.experimental.pallas import tpu as pltpu
from jax.sharding import PartitionSpec as P

epsilon = 1e-05
LANES = 128
FILLS = 4
NORMS = 8
EARLY = 4
BASES = (0.0, 2.0, 4.0, 6.0)
LANE, GROUP_AT, PLACE_AT, CORNER_AT, TIMES_AT, OWN = 1.5, 3.0, 2.0, 5.0, 7.0, -1.0
NORM_START, NORM_STEP = 0.2, 0.6
CORNER = (("y", "x", "y", "x"), ("x", "y", "x", "y"))
MESH = pl.DeviceIdType.MESH


def layout(mesh):
    sp, gr, tp = mesh.shape["sp"], mesh.shape["gr"], mesh.shape["tp"]
    inner = 1
    while inner * inner * 4 <= sp and sp % (inner * 2) == 0:
        inner *= 2
    return sp // inner, inner, gr, tp


def nearest(depth):
    return [[lane] + sorted((k for k in range(depth) if k != lane), key=lambda k: (abs(k - lane), -k)) for lane in range(depth)]


def plan(blocks, depth):
    steps = []
    for i in range(NORMS):
        steps.append((NORM_START + i * NORM_STEP, "norm", i))
    for m in range(blocks):
        base = BASES[m % len(BASES)]
        steps.append((-50.0 + 0.01 * m if m < EARLY else base + OWN, "own", m))
        for r in range(depth):
            at = base + r * LANE
            if r:
                steps.append((at, "lane", m, r))
                steps.append((at + GROUP_AT, "group", m, r))
            steps.append((at + PLACE_AT, "place", m, r))
            steps.append((at + CORNER_AT, "corner", m, r))
            end = max(at + TIMES_AT, NORM_START + NORMS * NORM_STEP)
            steps.append((end, "times", m, r))
        steps.append((end + 0.001, "trade", m))
    return sorted(steps, key=lambda step: step[0])


def body(
    grid, head_size,
    tokens, gain_in, w_key, w_value, queries_in, head_shift_in, key_shift_in,
    cache, read,
    raw, normed, weights, acc, outgoing, incoming, totals, parts,
    gain, queries, head_shift, key_shift,
    send_sem, piece_sem, cross_sem, last_sem, load_sem,
):
    depth, inner, groups, sections = grid
    seats = depth * inner
    seat, group, section = lax.axis_index("sp"), lax.axis_index("gr"), lax.axis_index("tp")
    lane, place = seat // inner, seat % inner
    rows, width = raw.shape
    shard, columns = w_key.shape
    blocks, _, span = weights.shape
    piece = shard // (groups * sections)
    kv_heads, heads = head_shift.shape
    seqs = seats // kv_heads
    sub = rows // seqs
    half = sub // 2
    per_kind = columns // span
    per_block = span // head_size
    fill_rows = rows // FILLS
    norm_rows = rows // NORMS

    own = pl.ds(pl.multiple_of(seat * shard, shard), shard)
    loads = []
    for m in range(blocks):
        source = (w_key, w_value)[m // per_kind].at[:, pl.ds((m % per_kind) * span, span)]
        loads.append(pltpu.make_async_copy(source, weights.at[m, own], load_sem.at[m]))
        loads[-1].start()
    fills = []
    for at in range(FILLS):
        rows_at = pl.ds(at * fill_rows, fill_rows)
        fills.append(pltpu.make_async_copy(tokens.at[rows_at], raw.at[rows_at], load_sem.at[blocks + at]))
        fills[-1].start()
    smalls = []
    for at, (source, target) in enumerate(
        ((gain_in, gain), (queries_in, queries), (head_shift_in, head_shift), (key_shift_in, key_shift))
    ):
        smalls.append(pltpu.make_async_copy(source, target, load_sem.at[blocks + FILLS + at]))
        smalls[-1].start()

    barrier = pltpu.get_barrier_semaphore()

    def greet(**where):
        pl.semaphore_signal(barrier, 1, device_id=where, device_id_type=MESH)

    @pl.when(lane > 0)
    def _():
        greet(sp=seat - inner)

    @pl.when(lane < depth - 1)
    def _():
        greet(sp=seat + inner)

    for j in range(1, inner):
        greet(sp=lane * inner + lax.rem(place + j, inner))
    for g in range(1, groups):
        greet(gr=lax.rem(group + g, groups))
    for t in range(1, sections):
        greet(tp=lax.rem(section + t, sections))

    order = nearest(depth)

    def lane_at(r):
        found = order[depth - 1][r]
        for k in range(depth - 1):
            differs = (lax.rem(lane - k + depth, depth) + depth - 1) // depth
            found = found + (1 - differs) * (order[k][r] - order[depth - 1][r])
        return found

    ranks = [lane] + [lane_at(r) for r in range(1, depth)]

    def piece_at(m, r, j, g):
        at = ranks[r] * inner + lax.rem(place + j, inner)
        share = lax.rem(group + g, groups) * sections + section
        start = pl.multiple_of(at * shard + share * piece, piece)
        return weights.at[m, pl.ds(start, piece)], piece_sem.at[m, at, lax.rem(group + g, groups)]

    sent = [0] * blocks

    def push(source, target, out_sem, in_sem, **where):
        pltpu.make_async_remote_copy(
            src_ref=source, dst_ref=target, send_sem=out_sem, recv_sem=in_sem, device_id=where, device_id_type=MESH
        ).start()

    def settle(like, sem):
        pltpu.make_async_copy(like, like, sem).wait()

    def to_places(m, r, g):
        block, sem = piece_at(m, r, 0, g)
        for j in range(1, inner):
            push(block, block, send_sem.at[m], sem, sp=lane * inner + lax.rem(place + j, inner))
            sent[m] += 1

    def to_groups(m, r, j):
        block, sem = piece_at(m, r, j, 0)
        for g in range(1, groups):
            push(block, block, send_sem.at[m], sem, gr=lax.rem(group + g, groups))
            sent[m] += 1

    def to_sections(m, r, j, g):
        block, _ = piece_at(m, r, j, g)
        for t in range(1, sections):
            push(block, block, send_sem.at[m], cross_sem.at[m, r], tp=lax.rem(section + t, sections))
            sent[m] += 1

    def arrive(m, r, j, g):
        settle(*piece_at(m, r, j, g))

    def step_own(m):
        loads[m].wait()
        block, sem = piece_at(m, 0, 0, 0)

        @pl.when(lane > 0)
        def _():
            push(block, block, send_sem.at[blocks + m], sem, sp=seat - inner)

        @pl.when(lane < depth - 1)
        def _():
            push(block, block, send_sem.at[blocks + m], sem, sp=seat + inner)

        to_places(m, 0, 0)
        if CORNER[m % len(CORNER)][0] == "y":
            for g in range(1, groups):
                to_places(m, 0, g)

    def step_lane(m, r):
        arrive(m, r, 0, 0)
        block, sem = piece_at(m, r, 0, 0)
        above = (ranks[r] - lane + depth) // depth
        onward = lane + 1 - 2 * above

        @pl.when((onward >= 0) & (onward < depth))
        def _():
            push(block, block, send_sem.at[blocks + m], sem, sp=onward * inner + place)

        to_places(m, r, 0)
        to_groups(m, r, 0)
        to_sections(m, r, 0, 0)

    def corner(m, r):
        return CORNER[m % len(CORNER)][min(r, len(CORNER[0]) - 1)]

    def step_group(m, r):
        for g in range(1, groups):
            arrive(m, r, 0, g)
            if corner(m, r) == "y":
                to_places(m, r, g)
            to_sections(m, r, 0, g)

    def step_place(m, r):
        for j in range(1, inner):
            arrive(m, r, j, 0)
            if corner(m, r) == "x":
                to_groups(m, r, j)
            to_sections(m, r, j, 0)

    def step_corner(m, r):
        for j in range(1, inner):
            for g in range(1, groups):
                arrive(m, r, j, g)
                to_sections(m, r, j, g)

    def step_norm(i):
        if i == 0:
            smalls[0].wait()
        if i * norm_rows % fill_rows == 0:
            fills[i * norm_rows // fill_rows].wait()
        step = 32

        @pl.loop(0, norm_rows // step)
        def _(k):
            here = pl.ds(pl.multiple_of(i * norm_rows + k * step, step), step)
            x = raw[here, :].astype(jnp.float32)
            mean = jnp.mean(x, axis=1, keepdims=True)
            centred = x - mean
            var = jnp.mean(centred * centred, axis=1, keepdims=True)
            scale = gain[...].astype(jnp.float32).reshape(1, width)
            normed[here, :] = (centred * lax.rsqrt(var + epsilon) * scale).astype(jnp.bfloat16)

    def step_times(m, r):
        count = ((inner - 1) if r == 0 else inner) * groups * (sections - 1)
        if count:
            settle(weights.at[m, pl.ds(0, count * piece)], cross_sem.at[m, r])
        long = inner * shard
        start = pl.multiple_of(ranks[r] * long, long)
        out = jnp.dot(normed[:, pl.ds(start, long)], weights[m, pl.ds(start, long), :], preferred_element_type=jnp.float32)
        if r == 0:
            acc[m] = out
        else:
            acc[m] += out

    def step_trade(m):
        kind, part = m // per_kind, m % per_kind
        for seq in range(seqs):
            for i in range(per_block):
                cut = slice(i * head_size, (i + 1) * head_size)
                first = acc[m, seq * sub:seq * sub + half, cut]
                second = acc[m, seq * sub + half:(seq + 1) * sub, cut]
                outgoing[m, seq * per_block + i] = jnp.concatenate([first, second], axis=1).astype(jnp.bfloat16)
        home = seat // kv_heads
        for s in range(seqs):
            seq = lax.rem(home + 1 + s, seqs)
            for i in range(per_block):
                to = seq * kv_heads + part * per_block + i
                at = seq * per_block + i

                def send():
                    push(outgoing.at[m, at], incoming.at[kind, seat], last_sem.at[kind], last_sem.at[2 + kind], sp=to)

                if s < seqs - 1:
                    send()
                else:
                    pl.when(to != seat)(send)

                    @pl.when(to == seat)
                    def _():
                        incoming[kind, pl.ds(seat, 1)] = outgoing[m, pl.ds(at, 1)]

    pl.semaphore_wait(barrier, inner + groups + sections - 3 + (lane + depth - 1) // depth + (2 * depth - 2 - lane) // depth)
    calls = {
        "own": step_own, "lane": step_lane, "group": step_group, "place": step_place, "corner": step_corner,
        "norm": step_norm, "times": step_times, "trade": step_trade,
    }
    for _, name, *arguments in plan(blocks, depth):
        with jax.named_scope(name + "_" + "_".join(map(str, arguments))):
            calls[name](*arguments)

    for copy in smalls[1:]:
        copy.wait()
    query = queries[...].astype(jnp.float32)
    query = jnp.concatenate([query[:, g * head_size:(g + 1) * head_size] for g in range(heads)], axis=0)
    blank = jnp.zeros_like(query)
    query = jnp.concatenate(
        [jnp.concatenate([query, blank], axis=1), jnp.concatenate([blank, query], axis=1)], axis=0
    ).astype(jnp.bfloat16)
    mine = lax.broadcasted_iota(jnp.int32, (kv_heads, heads), 0) == lax.rem(seat, kv_heads)
    shift = jnp.sum(jnp.where(mine, head_shift[...], 0.0), axis=0, keepdims=True)
    eye = lax.broadcasted_iota(jnp.int32, (heads, heads), 0) == lax.broadcasted_iota(jnp.int32, (heads, heads), 1)
    shift = jnp.sum(jnp.where(eye, jnp.broadcast_to(shift, (heads, heads)), 0.0), axis=1, keepdims=True)
    later = (
        lax.broadcasted_iota(jnp.int32, (half, half), 0) > lax.broadcasted_iota(jnp.int32, (half, half), 1)
    ).astype(jnp.float32)

    with jax.named_scope("keys_in"):
        settle(incoming.at[0, pl.ds(0, seats - 1)], last_sem.at[2])
    trace = jax.named_scope("logits")
    trace.__enter__()
    keys = incoming[0].reshape(seats * half, 2 * head_size)
    logits = lax.dot_general(query, keys, (((1,), (1,)), ((), ())), preferred_element_type=jnp.float32)
    logits = logits * head_size ** (-0.5)
    betas, keeps = [], []
    for at in range(2 * seats):
        q, h = at // 2, at % 2
        z = logits[h * heads:(h + 1) * heads, q * half:(q + 1) * half]
        z = z + shift + key_shift[:, at * half:(at + 1) * half]
        tail = jnp.log1p(jnp.exp(-jnp.abs(z)))
        betas.append(jnp.minimum(z, 0.0) - tail)
        keeps.append(jnp.minimum(-z, 0.0) - tail)
    within = jnp.dot(
        jnp.concatenate(keeps, axis=0), later, preferred_element_type=jnp.float32, precision=lax.Precision.HIGHEST
    )
    running = jnp.zeros((heads, 1), jnp.float32)
    local = [None] * (2 * seats)
    for at in reversed(range(2 * seats)):
        local[at] = jnp.exp(betas[at] + within[at * heads:(at + 1) * heads] + running)
        running = running + jnp.sum(keeps[at], axis=1, keepdims=True)
    local = jnp.concatenate(
        [jnp.concatenate(local[0::2], axis=1), jnp.concatenate(local[1::2], axis=1)], axis=0
    ).astype(jnp.bfloat16)
    totals[section] = jnp.broadcast_to(running, totals.shape[1:])
    for t in range(1, sections):
        push(totals.at[section], totals.at[section], last_sem.at[4], last_sem.at[5], tp=lax.rem(section + t, sections))
    trace.__exit__(None, None, None)
    trace = jax.named_scope("totals_in")
    trace.__enter__()
    if sections > 1:
        settle(totals.at[pl.ds(0, sections - 1)], last_sem.at[5])
    carry = jnp.zeros((heads, head_size), jnp.float32)
    for t in reversed(range(sections)):
        carry = carry + jnp.where(section < t, totals[t][:, :head_size], 0.0)
    carry = jnp.exp(carry)
    trace.__exit__(None, None, None)

    with jax.named_scope("values_in"):
        settle(incoming.at[1, pl.ds(0, seats - 1)], last_sem.at[3])
    trace = jax.named_scope("part")
    trace.__enter__()
    values = incoming[1].reshape(seats * half, 2 * head_size)
    part = jnp.dot(local, values, preferred_element_type=jnp.float32)
    part = carry * (part[:heads, :head_size] + part[heads:, head_size:])
    parts[section] = jnp.concatenate([part, part], axis=1)
    for t in range(1, sections):
        push(parts.at[section], parts.at[section], last_sem.at[6], last_sem.at[7], tp=lax.rem(section + t, sections))
    trace.__exit__(None, None, None)
    trace = jax.named_scope("cache")
    trace.__enter__()
    for q in range(seats):
        for h in range(2):
            cut = slice(h * head_size, (h + 1) * head_size)
            start = (2 * q + h) * half
            cache[0, start:start + half, :] = jnp.concatenate([incoming[0, q][:, cut], incoming[1, q][:, cut]], axis=1)
    for m in range(blocks):
        settle(weights.at[m, pl.ds(0, sent[m] * piece)], send_sem.at[m])
        for k in range(depth):
            count = (k + 1 if k < depth - 1 else 0) + (depth - k if k > 0 else 0)
            if count:
                @pl.when(lane == k)
                def _():
                    settle(weights.at[m, pl.ds(0, count * piece)], send_sem.at[blocks + m])
    for kind in range(2):
        settle(incoming.at[kind, pl.ds(0, seats - 1)], last_sem.at[kind])
    trace.__exit__(None, None, None)
    trace = jax.named_scope("parts_in")
    trace.__enter__()
    if sections > 1:
        settle(totals.at[pl.ds(0, sections - 1)], last_sem.at[4])
        settle(parts.at[pl.ds(0, sections - 1)], last_sem.at[6])
        settle(parts.at[pl.ds(0, sections - 1)], last_sem.at[7])
    total = parts[0]
    for t in range(1, sections):
        total = total + parts[t]
    for g in range(heads):
        read[:, g * head_size:(g + 1) * head_size] = total[g:g + 1, :head_size]
    trace.__exit__(None, None, None)


def hand_over(cache, read, cache_out, read_out, sem):
    first = pltpu.make_async_copy(cache, cache_out, sem.at[0])
    second = pltpu.make_async_copy(read, read_out, sem.at[1])
    first.start()
    second.start()
    first.wait()
    second.wait()


def local(grid, tokens, ln_gain, w_key, w_value, queries, head_shift, key_shift):
    depth, inner, groups, sections = grid
    seats = depth * inner
    seqs, _, sub, width = tokens.shape
    rows = seqs * sub
    columns = w_key.shape[1]
    kv_heads, heads = head_shift.shape
    head_size = columns // kv_heads
    blocks = 2 * columns // LANES
    vmem = pl.BlockSpec(memory_space=pltpu.VMEM)
    hbm = pl.BlockSpec(memory_space=pl.ANY)
    operands = (tokens.reshape(rows, width), ln_gain, w_key, w_value, queries, head_shift, key_shift)
    cache, read = pl.pallas_call(
        functools.partial(body, grid, head_size),
        out_shape=(
            jax.ShapeDtypeStruct((1, seats * sub, 2 * head_size), jnp.bfloat16),
            jax.ShapeDtypeStruct((1, heads * head_size), jnp.float32),
        ),
        in_specs=[hbm] * len(operands),
        out_specs=(vmem, vmem),
        scratch_shapes=[
            pltpu.VMEM((rows, width), jnp.bfloat16),
            pltpu.VMEM((rows, width), jnp.bfloat16),
            pltpu.VMEM((blocks, width, LANES), jnp.bfloat16),
            pltpu.VMEM((blocks, rows, LANES), jnp.float32),
            pltpu.VMEM((blocks, seqs * LANES // head_size, sub // 2, 2 * head_size), jnp.bfloat16),
            pltpu.VMEM((2, seats, sub // 2, 2 * head_size), jnp.bfloat16),
            pltpu.VMEM((sections, heads, 2 * head_size), jnp.float32),
            pltpu.VMEM((sections, heads, 2 * head_size), jnp.float32),
            pltpu.VMEM(ln_gain.shape, ln_gain.dtype),
            pltpu.VMEM(queries.shape, queries.dtype),
            pltpu.VMEM(head_shift.shape, head_shift.dtype),
            pltpu.VMEM(key_shift.shape, key_shift.dtype),
            pltpu.SemaphoreType.DMA((2 * blocks,)),
            pltpu.SemaphoreType.DMA((blocks, seats, groups)),
            pltpu.SemaphoreType.DMA((blocks, depth)),
            pltpu.SemaphoreType.DMA((8,)),
            pltpu.SemaphoreType.DMA((blocks + FILLS + 4,)),
        ],
        compiler_params=pltpu.CompilerParams(
            collective_id=0, has_side_effects=True, vmem_limit_bytes=24 * 1024 * 1024
        ),
    )(*(pltpu.with_memory_space_constraint(x, pltpu.HBM) for x in operands))
    return pl.pallas_call(
        hand_over,
        out_shape=(jax.ShapeDtypeStruct(cache.shape, cache.dtype), jax.ShapeDtypeStruct(read.shape, read.dtype)),
        in_specs=[vmem, vmem],
        out_specs=(hbm, hbm),
        scratch_shapes=[pltpu.SemaphoreType.DMA((2,))],
        compiler_params=pltpu.CompilerParams(vmem_limit_bytes=4 * 1024 * 1024),
    )(cache, read)


def solution(mesh):
    in_specs = (
        P("gr", "tp", "sp", None),
        P(),
        P("sp", None),
        P("sp", None),
        P(("gr", "sp"), None),
        P(),
        P(("gr", "sp"), "tp"),
    )
    out_specs = (P(("gr", "sp"), "tp", None), P(("gr", "sp"), None))
    return jax.shard_map(
        functools.partial(local, layout(mesh)), mesh=mesh, in_specs=in_specs, out_specs=out_specs, check_vma=False
    )
```

time: 46.9 us -> 42.6 us (0.908)
  Pallas kernels: 45.8 us -> 41.6 us
    pallas_call x1, Pallas kernels: 43.9 us -> 40.7 us  [local(): pl.pallas_call(functools.partial(body, grid, head_size), out_shape=(jax.S...]
    pallas_call x1, Pallas kernels: 1.87 us -> 0.81 us  [local(): pl.pallas_call(hand_over, out_shape=(jax.ShapeDtypeStruct(cache.shape, ca...]
where the time goes in v1:
time: 42.6 us; the launch traced here: 42.2 us
  Pallas kernels  41.6 us (98%)
  between operations  0.64 us (2%)
    pallas_call x1, Pallas kernels, local(): pl.pallas_call(functools.partial(body, grid, head_size), out_shape=(jax.S...  40.7 us

profile of v1, /device:TPU:13, one launch (start us, length us, event | category | flops | bytes accessed | tf_op | source)
XLA Modules:
  0.0 42.2 jit_solution(9992783457829347814)
XLA Ops:
  0.6 40.7 %shard_map.86 = (bf16[1,2048,128]{2,1,0:T(8,128)(2,1)S(1)}, f32[1,512]{1,0:T(1,128)S(1)}) custom-call(bf16[512,4096]{1,0:T(8,128)(2,1)} %bitcast.1, bf16[4096]{0:T(1024)(128)(2,1)} %gain_in.1, bf16[512,256]{1,0:T(8,128)(2,1)} %w_key.1, bf16[512,256]{1,0:T(8,128)(2,1)} %w_value.1, bf16[1,512]{1,0:T(2,128)(2,1)} %queries_in.1, f32[4,8]{1,0:T(4,128)} %head_shift_in.1, ...), custom_call_target="tpu_custom_call" | custom-call | tf_op jit(solution)/shard_map/pallas_call | solution.py:404
  41.4 0.8 %shard_map.87 = (bf16[1,2048,128]{2,1,0:T(8,128)(2,1)}, f32[1,512]{1,0:T(1,128)}) custom-call(bf16[1,2048,128]{2,1,0:T(8,128)(2,1)S(1)} %get-tuple-element.4.cache, f32[1,512]{1,0:T(1,128)S(1)} %get-tuple-element.5.read), custom_call_target="tpu_custom_call" | custom-call | tf_op jit(solution)/shard_map/pallas_call | solution.py:435

commit v2 on v1

--- a/solution.py
+++ b/solution.py
@@ -9,13 +9,30 @@
 
 epsilon = 1e-05
 LANES = 128
+NORM, OWN, HOP, GROUP, PLACE, EDGE, TIMES, PAIR, TRADE = range(9)
 FILLS = 4
 NORMS = 8
-EARLY = 4
 BASES = (0.0, 2.0, 4.0, 6.0)
-LANE, GROUP_AT, PLACE_AT, CORNER_AT, TIMES_AT, OWN = 1.5, 3.0, 2.0, 5.0, 7.0, -1.0
+LANE_STEP, GROUP_AT, PLACE_AT, CORNER_AT, TIMES_AT, OWN_AT = 1.5, 3.0, 2.0, 5.0, 7.0, -3.0
 NORM_START, NORM_STEP = 0.2, 0.6
-CORNER = (("y", "x", "y", "x"), ("x", "y", "x", "y"))
+CORNER = (("y", "y", "y", "y"), ("x", "x", "y", "x"), ("x", "x", "y", "x"), ("x", "x", "x", "x"))
+ORDER = (
+    (OWN, 0, 0), (NORM, 4, 0), (OWN, 1, 0), (OWN, 2, 0), (OWN, 3, 0), (NORM, 7, 0),
+    (NORM, 5, 0), (NORM, 2, 0), (HOP, 0, 2), (HOP, 0, 1), (HOP, 1, 2), (HOP, 1, 1),
+    (PLACE, 2, 0), (PLACE, 0, 0), (GROUP, 0, 1), (HOP, 0, 3), (GROUP, 0, 2), (HOP, 1, 3),
+    (HOP, 2, 1), (NORM, 6, 0), (NORM, 1, 0), (PLACE, 1, 1), (PLACE, 0, 1), (PLACE, 0, 2),
+    (GROUP, 0, 3), (HOP, 2, 2), (GROUP, 1, 2), (NORM, 3, 0), (PLACE, 1, 0), (GROUP, 1, 1),
+    (NORM, 0, 0), (HOP, 2, 3), (EDGE, 0, 0), (PLACE, 1, 3), (EDGE, 0, 1), (PLACE, 0, 3),
+    (EDGE, 0, 2), (PLACE, 2, 1), (HOP, 3, 1), (EDGE, 0, 3), (HOP, 3, 2), (GROUP, 2, 2),
+    (GROUP, 1, 3), (TIMES, 0, 0), (EDGE, 1, 0), (GROUP, 2, 1), (EDGE, 1, 1), (PLACE, 1, 2),
+    (EDGE, 2, 0), (EDGE, 1, 2), (PLACE, 2, 3), (TIMES, 0, 1), (TIMES, 0, 3), (EDGE, 1, 3),
+    (HOP, 3, 3), (TIMES, 0, 2), (TRADE, 0, 0), (GROUP, 3, 1), (PLACE, 2, 2), (TIMES, 1, 0),
+    (PLACE, 3, 1), (PLACE, 3, 2), (EDGE, 2, 1), (TIMES, 1, 1), (EDGE, 2, 2), (GROUP, 2, 3),
+    (TIMES, 1, 2), (TIMES, 1, 3), (PLACE, 3, 0), (EDGE, 2, 3), (TRADE, 1, 0), (TIMES, 2, 1),
+    (PLACE, 3, 3), (TIMES, 2, 2), (GROUP, 3, 2), (TIMES, 2, 0), (EDGE, 3, 0), (TIMES, 2, 3),
+    (TRADE, 2, 0), (EDGE, 3, 1), (EDGE, 3, 3), (GROUP, 3, 3), (EDGE, 3, 2), (TIMES, 3, 2),
+    (TIMES, 3, 3), (TIMES, 3, 1), (TIMES, 3, 0), (TRADE, 3, 0),
+)
 MESH = pl.DeviceIdType.MESH
 
 
@@ -32,23 +49,25 @@
 
 
 def plan(blocks, depth):
+    if (blocks, depth) == (len(CORNER), len(CORNER[0])):
+        return ORDER
     steps = []
     for i in range(NORMS):
-        steps.append((NORM_START + i * NORM_STEP, "norm", i))
+        steps.append((NORM_START + i * NORM_STEP, NORM, i, 0))
     for m in range(blocks):
         base = BASES[m % len(BASES)]
-        steps.append((-50.0 + 0.01 * m if m < EARLY else base + OWN, "own", m))
+        steps.append((base + OWN_AT, OWN, m, 0))
         for r in range(depth):
-            at = base + r * LANE
+            at = base + r * LANE_STEP
             if r:
-                steps.append((at, "lane", m, r))
-                steps.append((at + GROUP_AT, "group", m, r))
-            steps.append((at + PLACE_AT, "place", m, r))
-            steps.append((at + CORNER_AT, "corner", m, r))
+                steps.append((at, HOP, m, r))
+                steps.append((at + GROUP_AT, GROUP, m, r))
+            steps.append((at + PLACE_AT, PLACE, m, r))
+            steps.append((at + CORNER_AT, EDGE, m, r))
             end = max(at + TIMES_AT, NORM_START + NORMS * NORM_STEP)
-            steps.append((end, "times", m, r))
-        steps.append((end + 0.001, "trade", m))
-    return sorted(steps, key=lambda step: step[0])
+            steps.append((end, TIMES, m, r))
+        steps.append((end + 0.001, TRADE, m, 0))
+    return [step[1:] for step in sorted(steps, key=lambda step: step[0])]
 
 
 def body(
@@ -162,7 +181,7 @@
     def arrive(m, r, j, g):
         settle(*piece_at(m, r, j, g))
 
-    def step_own(m):
+    def step_own(m, _):
         loads[m].wait()
         block, sem = piece_at(m, 0, 0, 0)
 
@@ -216,11 +235,22 @@
                 arrive(m, r, j, g)
                 to_sections(m, r, j, g)
 
-    def step_norm(i):
-        if i == 0:
+    filled, begun = set(), set()
+
+    def add(m, out):
+        if m in begun:
+            acc[m] += out
+        else:
+            acc[m] = out
+            begun.add(m)
+
+    def step_norm(i, _):
+        if not filled:
             smalls[0].wait()
-        if i * norm_rows % fill_rows == 0:
-            fills[i * norm_rows // fill_rows].wait()
+        stage = i * norm_rows // fill_rows
+        if stage not in filled:
+            fills[stage].wait()
+            filled.add(stage)
         step = 32
 
         @pl.loop(0, norm_rows // step)
@@ -233,19 +263,29 @@
             scale = gain[...].astype(jnp.float32).reshape(1, width)
             normed[here, :] = (centred * lax.rsqrt(var + epsilon) * scale).astype(jnp.bfloat16)
 
-    def step_times(m, r):
+    def crossed(m, r):
         count = ((inner - 1) if r == 0 else inner) * groups * (sections - 1)
         if count:
             settle(weights.at[m, pl.ds(0, count * piece)], cross_sem.at[m, r])
+
+    def step_pair(k, r):
+        crossed(2 * k, r)
+        crossed(2 * k + 1, r)
+        long = inner * shard
+        start = pl.multiple_of(ranks[r] * long, long)
+        both = jnp.concatenate([weights[2 * k, pl.ds(start, long), :], weights[2 * k + 1, pl.ds(start, long), :]], axis=1)
+        out = jnp.dot(normed[:, pl.ds(start, long)], both, preferred_element_type=jnp.float32)
+        for m in range(2):
+            add(2 * k + m, out[:, m * span:(m + 1) * span])
+
+    def step_times(m, r):
+        crossed(m, r)
         long = inner * shard
         start = pl.multiple_of(ranks[r] * long, long)
         out = jnp.dot(normed[:, pl.ds(start, long)], weights[m, pl.ds(start, long), :], preferred_element_type=jnp.float32)
-        if r == 0:
-            acc[m] = out
-        else:
-            acc[m] += out
-
-    def step_trade(m):
+        add(m, out)
+
+    def step_trade(m, _):
         kind, part = m // per_kind, m % per_kind
         for seq in range(seqs):
             for i in range(per_block):
@@ -273,13 +313,10 @@
                         incoming[kind, pl.ds(seat, 1)] = outgoing[m, pl.ds(at, 1)]
 
     pl.semaphore_wait(barrier, inner + groups + sections - 3 + (lane + depth - 1) // depth + (2 * depth - 2 - lane) // depth)
-    calls = {
-        "own": step_own, "lane": step_lane, "group": step_group, "place": step_place, "corner": step_corner,
-        "norm": step_norm, "times": step_times, "trade": step_trade,
-    }
-    for _, name, *arguments in plan(blocks, depth):
-        with jax.named_scope(name + "_" + "_".join(map(str, arguments))):
-            calls[name](*arguments)
+    calls = (step_norm, step_own, step_lane, step_group, step_place, step_corner, step_times, step_pair, step_trade)
+    for which, m, r in plan(blocks, depth):
+        with jax.named_scope(f"{calls[which].__name__}_{m}_{r}"):
+            calls[which](m, r)
 
     for copy in smalls[1:]:
         copy.wait()

time: 42.6 us -> 41.1 us (0.965)
  Pallas kernels: 41.6 us -> 40.3 us
    pallas_call x1, Pallas kernels: 40.7 us -> 39.5 us  [local(): pl.pallas_call(functools.partial(body, grid, head_size), out_shape=(jax.S...]
where the time goes in v2:
time: 41.1 us; the launch traced here: 40.9 us
  Pallas kernels  40.3 us (98%)
  between operations  0.64 us (2%)
    pallas_call x1, Pallas kernels, local(): pl.pallas_call(functools.partial(body, grid, head_size), out_shape=(jax.S...  39.5 us

profile of v2, /device:TPU:13, one launch (start us, length us, event | category | flops | bytes accessed | tf_op | source)
XLA Modules:
  0.0 40.9 jit_solution(5672565103661661673)
XLA Ops:
  0.6 39.5 %shard_map.86 = (bf16[1,2048,128]{2,1,0:T(8,128)(2,1)S(1)}, f32[1,512]{1,0:T(1,128)S(1)}) custom-call(bf16[512,4096]{1,0:T(8,128)(2,1)} %bitcast.1, bf16[4096]{0:T(1024)(128)(2,1)} %gain_in.1, bf16[512,256]{1,0:T(8,128)(2,1)} %w_key.1, bf16[512,256]{1,0:T(8,128)(2,1)} %w_value.1, bf16[1,512]{1,0:T(2,128)(2,1)} %queries_in.1, f32[4,8]{1,0:T(4,128)} %head_shift_in.1, ...), custom_call_target="tpu_custom_call" | custom-call | tf_op jit(solution)/shard_map/pallas_call | solution.py:441
  40.1 0.8 %shard_map.87 = (bf16[1,2048,128]{2,1,0:T(8,128)(2,1)}, f32[1,512]{1,0:T(1,128)}) custom-call(bf16[1,2048,128]{2,1,0:T(8,128)(2,1)S(1)} %get-tuple-element.4.cache, f32[1,512]{1,0:T(1,128)S(1)} %get-tuple-element.5.read), custom_call_target="tpu_custom_call" | custom-call | tf_op jit(solution)/shard_map/pallas_call | solution.py:472

commit v3 on v2

--- a/solution.py
+++ b/solution.py
@@ -15,23 +15,24 @@
 BASES = (0.0, 2.0, 4.0, 6.0)
 LANE_STEP, GROUP_AT, PLACE_AT, CORNER_AT, TIMES_AT, OWN_AT = 1.5, 3.0, 2.0, 5.0, 7.0, -3.0
 NORM_START, NORM_STEP = 0.2, 0.6
-CORNER = (("y", "y", "y", "y"), ("x", "x", "y", "x"), ("x", "x", "y", "x"), ("x", "x", "x", "x"))
+CORNER = (("y", "x", "x", "x"), ("y", "y", "x", "x"), ("x", "y", "y", "x"), ("x", "x", "y", "x"))
+OUTER = (False, False, True, True)
 ORDER = (
-    (OWN, 0, 0), (NORM, 4, 0), (OWN, 1, 0), (OWN, 2, 0), (OWN, 3, 0), (NORM, 7, 0),
-    (NORM, 5, 0), (NORM, 2, 0), (HOP, 0, 2), (HOP, 0, 1), (HOP, 1, 2), (HOP, 1, 1),
-    (PLACE, 2, 0), (PLACE, 0, 0), (GROUP, 0, 1), (HOP, 0, 3), (GROUP, 0, 2), (HOP, 1, 3),
-    (HOP, 2, 1), (NORM, 6, 0), (NORM, 1, 0), (PLACE, 1, 1), (PLACE, 0, 1), (PLACE, 0, 2),
-    (GROUP, 0, 3), (HOP, 2, 2), (GROUP, 1, 2), (NORM, 3, 0), (PLACE, 1, 0), (GROUP, 1, 1),
-    (NORM, 0, 0), (HOP, 2, 3), (EDGE, 0, 0), (PLACE, 1, 3), (EDGE, 0, 1), (PLACE, 0, 3),
-    (EDGE, 0, 2), (PLACE, 2, 1), (HOP, 3, 1), (EDGE, 0, 3), (HOP, 3, 2), (GROUP, 2, 2),
-    (GROUP, 1, 3), (TIMES, 0, 0), (EDGE, 1, 0), (GROUP, 2, 1), (EDGE, 1, 1), (PLACE, 1, 2),
-    (EDGE, 2, 0), (EDGE, 1, 2), (PLACE, 2, 3), (TIMES, 0, 1), (TIMES, 0, 3), (EDGE, 1, 3),
-    (HOP, 3, 3), (TIMES, 0, 2), (TRADE, 0, 0), (GROUP, 3, 1), (PLACE, 2, 2), (TIMES, 1, 0),
-    (PLACE, 3, 1), (PLACE, 3, 2), (EDGE, 2, 1), (TIMES, 1, 1), (EDGE, 2, 2), (GROUP, 2, 3),
-    (TIMES, 1, 2), (TIMES, 1, 3), (PLACE, 3, 0), (EDGE, 2, 3), (TRADE, 1, 0), (TIMES, 2, 1),
-    (PLACE, 3, 3), (TIMES, 2, 2), (GROUP, 3, 2), (TIMES, 2, 0), (EDGE, 3, 0), (TIMES, 2, 3),
-    (TRADE, 2, 0), (EDGE, 3, 1), (EDGE, 3, 3), (GROUP, 3, 3), (EDGE, 3, 2), (TIMES, 3, 2),
-    (TIMES, 3, 3), (TIMES, 3, 1), (TIMES, 3, 0), (TRADE, 3, 0),
+    (OWN, 0, 0), (OWN, 1, 0), (NORM, 7, 0), (OWN, 3, 0), (OWN, 2, 0), (NORM, 2, 0),
+    (HOP, 0, 1), (NORM, 5, 0), (HOP, 1, 1), (HOP, 0, 2), (EDGE, 1, 0), (HOP, 0, 3),
+    (HOP, 1, 2), (NORM, 0, 0), (HOP, 1, 3), (GROUP, 3, 1), (NORM, 4, 0), (HOP, 2, 1),
+    (GROUP, 1, 1), (GROUP, 0, 1), (PLACE, 0, 2), (PLACE, 0, 1), (NORM, 3, 0), (EDGE, 0, 0),
+    (GROUP, 0, 2), (HOP, 3, 1), (HOP, 2, 2), (PLACE, 1, 1), (PLACE, 0, 3), (NORM, 6, 0),
+    (HOP, 2, 3), (PLACE, 2, 0), (PLACE, 1, 2), (NORM, 1, 0), (PLACE, 1, 3), (PLACE, 1, 0),
+    (TIMES, 1, 0), (PLACE, 3, 0), (EDGE, 0, 2), (TIMES, 0, 2), (EDGE, 0, 1), (GROUP, 1, 3),
+    (GROUP, 2, 1), (TIMES, 0, 1), (HOP, 3, 2), (GROUP, 0, 3), (PLACE, 0, 0), (TIMES, 0, 0),
+    (GROUP, 2, 2), (EDGE, 1, 1), (HOP, 3, 3), (PLACE, 2, 1), (EDGE, 0, 3), (TIMES, 0, 3),
+    (TRADE, 0, 0), (EDGE, 1, 2), (EDGE, 2, 1), (TIMES, 1, 1), (GROUP, 2, 3), (EDGE, 1, 3),
+    (EDGE, 2, 0), (GROUP, 1, 2), (PLACE, 2, 3), (PLACE, 3, 2), (PLACE, 3, 1), (TIMES, 1, 3),
+    (EDGE, 2, 2), (EDGE, 3, 0), (PLACE, 2, 2), (TIMES, 1, 2), (TRADE, 1, 0), (TIMES, 3, 0),
+    (GROUP, 3, 2), (TIMES, 2, 1), (PLACE, 3, 3), (TIMES, 2, 2), (GROUP, 3, 3), (EDGE, 2, 3),
+    (TIMES, 2, 0), (TIMES, 2, 3), (TRADE, 2, 0), (EDGE, 3, 1), (TIMES, 3, 1), (EDGE, 3, 3),
+    (TIMES, 3, 3), (EDGE, 3, 2), (TIMES, 3, 2), (TRADE, 3, 0),
 )
 MESH = pl.DeviceIdType.MESH
 
@@ -45,7 +46,7 @@
 
 
 def nearest(depth):
-    return [[lane] + sorted((k for k in range(depth) if k != lane), key=lambda k: (abs(k - lane), -k)) for lane in range(depth)]
+    return [[lane] + sorted((k for k in range(depth) if k != lane), key=lambda k: (abs(k - lane), k if 2 * lane < depth else -k)) for lane in range(depth)]
 
 
 def plan(blocks, depth):
@@ -85,7 +86,9 @@
     rows, width = raw.shape
     shard, columns = w_key.shape
     blocks, _, span = weights.shape
-    piece = shard // (groups * sections)
+    leads = sections if sections > 2 else 1
+    leading = section == sections - 1
+    piece = shard // (groups * leads)
     kv_heads, heads = head_shift.shape
     seqs = seats // kv_heads
     sub = rows // seqs
@@ -146,7 +149,7 @@
 
     def piece_at(m, r, j, g):
         at = ranks[r] * inner + lax.rem(place + j, inner)
-        share = lax.rem(group + g, groups) * sections + section
+        share = lax.rem(group + g, groups) * leads + (section if leads > 1 else 0)
         start = pl.multiple_of(at * shard + share * piece, piece)
         return weights.at[m, pl.ds(start, piece)], piece_sem.at[m, at, lax.rem(group + g, groups)]
 
@@ -159,6 +162,19 @@
 
     def settle(like, sem):
         pltpu.make_async_copy(like, like, sem).wait()
+
+    def settle_pieces(count, sem):
+        total = count * piece
+        if total <= width:
+            settle(weights.at[0, pl.ds(0, total)], sem)
+        else:
+            settle(raw.at[pl.ds(0, total * span // width)], sem)
+
+    def lead(step):
+        if leads == 1:
+            pl.when(leading)(step)
+        else:
+            step()
 
     def to_places(m, r, g):
         block, sem = piece_at(m, r, 0, g)
@@ -178,11 +194,17 @@
             push(block, block, send_sem.at[m], cross_sem.at[m, r], tp=lax.rem(section + t, sections))
             sent[m] += 1
 
+    def outer(m):
+        return depth == 4 and OUTER[m % len(OUTER)]
+
     def arrive(m, r, j, g):
         settle(*piece_at(m, r, j, g))
 
     def step_own(m, _):
         loads[m].wait()
+        lead(lambda: send_own(m))
+
+    def send_own(m):
         block, sem = piece_at(m, 0, 0, 0)
 
         @pl.when(lane > 0)
@@ -193,6 +215,11 @@
         def _():
             push(block, block, send_sem.at[blocks + m], sem, sp=seat + inner)
 
+        if outer(m):
+            for g in range(1, groups):
+                other, its_sem = piece_at(m, 0, 0, g)
+                across = lane + 1 - 2 * lax.rem(lane, 2)
+                push(other, other, send_sem.at[blocks + m], its_sem, sp=across * inner + place)
         to_places(m, 0, 0)
         if CORNER[m % len(CORNER)][0] == "y":
             for g in range(1, groups):
@@ -209,7 +236,8 @@
             push(block, block, send_sem.at[blocks + m], sem, sp=onward * inner + place)
 
         to_places(m, r, 0)
-        to_groups(m, r, 0)
+        if not (outer(m) and r == 1):
+            to_groups(m, r, 0)
         to_sections(m, r, 0, 0)
 
     def corner(m, r):
@@ -264,9 +292,12 @@
             normed[here, :] = (centred * lax.rsqrt(var + epsilon) * scale).astype(jnp.bfloat16)
 
     def crossed(m, r):
-        count = ((inner - 1) if r == 0 else inner) * groups * (sections - 1)
-        if count:
-            settle(weights.at[m, pl.ds(0, count * piece)], cross_sem.at[m, r])
+        count = ((inner - 1) if r == 0 else inner) * groups * (sections - 1 if leads > 1 else 1)
+        if count and sections > 1:
+            if leads > 1:
+                settle_pieces(count, cross_sem.at[m, r])
+            else:
+                pl.when(section != sections - 1)(lambda: settle_pieces(count, cross_sem.at[m, r]))
 
     def step_pair(k, r):
         crossed(2 * k, r)
@@ -316,7 +347,10 @@
     calls = (step_norm, step_own, step_lane, step_group, step_place, step_corner, step_times, step_pair, step_trade)
     for which, m, r in plan(blocks, depth):
         with jax.named_scope(f"{calls[which].__name__}_{m}_{r}"):
-            calls[which](m, r)
+            if HOP <= which <= EDGE:
+                lead(lambda: calls[which](m, r))
+            else:
+                calls[which](m, r)
 
     for copy in smalls[1:]:
         copy.wait()
@@ -392,14 +426,15 @@
             cut = slice(h * head_size, (h + 1) * head_size)
             start = (2 * q + h) * half
             cache[0, start:start + half, :] = jnp.concatenate([incoming[0, q][:, cut], incoming[1, q][:, cut]], axis=1)
-    for m in range(blocks):
-        settle(weights.at[m, pl.ds(0, sent[m] * piece)], send_sem.at[m])
-        for k in range(depth):
-            count = (k + 1 if k < depth - 1 else 0) + (depth - k if k > 0 else 0)
-            if count:
-                @pl.when(lane == k)
-                def _():
-                    settle(weights.at[m, pl.ds(0, count * piece)], send_sem.at[blocks + m])
+    def drain():
+        for m in range(blocks):
+            settle_pieces(sent[m], send_sem.at[m])
+            for k in range(depth):
+                count = (k + 1 if k < depth - 1 else 0) + (depth - k if k > 0 else 0) + (groups - 1) * outer(m)
+                if count:
+                    pl.when(lane == k)(lambda count=count: settle_pieces(count, send_sem.at[blocks + m]))
+
+    lead(drain)
     for kind in range(2):
         settle(incoming.at[kind, pl.ds(0, seats - 1)], last_sem.at[kind])
     trace.__exit__(None, None, None)

time: 41.1 us -> 37.1 us (0.903)
  Pallas kernels: 40.3 us -> 36.3 us
    pallas_call x1, Pallas kernels: 39.5 us -> 35.5 us  [local(): pl.pallas_call(functools.partial(body, grid, head_size), out_shape=(jax.S...]
where the time goes in v3:
time: 37.1 us; the launch traced here: 37 us
  Pallas kernels  36.3 us (98%)
  between operations  0.64 us (2%)
    pallas_call x1, Pallas kernels, local(): pl.pallas_call(functools.partial(body, grid, head_size), out_shape=(jax.S...  35.5 us
    pallas_call x1, Pallas kernels, local(): pl.pallas_call(hand_over, out_shape=(jax.ShapeDtypeStruct(cache.shape, ca...  0.81 us

profile of v3, /device:TPU:13, one launch (start us, length us, event | category | flops | bytes accessed | tf_op | source)
XLA Modules:
  0.0 37.0 jit_solution(17772464390696679514)
XLA Ops:
  0.6 35.5 %shard_map.86 = (bf16[1,2048,128]{2,1,0:T(8,128)(2,1)S(1)}, f32[1,512]{1,0:T(1,128)S(1)}) custom-call(bf16[512,4096]{1,0:T(8,128)(2,1)} %bitcast.1, bf16[4096]{0:T(1024)(128)(2,1)} %gain_in.1, bf16[512,256]{1,0:T(8,128)(2,1)} %w_key.1, bf16[512,256]{1,0:T(8,128)(2,1)} %w_value.1, bf16[1,512]{1,0:T(2,128)(2,1)} %queries_in.1, f32[4,8]{1,0:T(4,128)} %head_shift_in.1, ...), custom_call_target="tpu_custom_call" | custom-call | tf_op jit(solution)/shard_map/pallas_call | solution.py:476
  36.2 0.8 %shard_map.87 = (bf16[1,2048,128]{2,1,0:T(8,128)(2,1)}, f32[1,512]{1,0:T(1,128)}) custom-call(bf16[1,2048,128]{2,1,0:T(8,128)(2,1)S(1)} %get-tuple-element.4.cache, f32[1,512]{1,0:T(1,128)S(1)} %get-tuple-element.5.read), custom_call_target="tpu_custom_call" | custom-call | tf_op jit(solution)/shard_map/pallas_call | solution.py:507

commit v4 on v3

--- a/solution.py
+++ b/solution.py
@@ -15,24 +15,24 @@
 BASES = (0.0, 2.0, 4.0, 6.0)
 LANE_STEP, GROUP_AT, PLACE_AT, CORNER_AT, TIMES_AT, OWN_AT = 1.5, 3.0, 2.0, 5.0, 7.0, -3.0
 NORM_START, NORM_STEP = 0.2, 0.6
-CORNER = (("y", "x", "x", "x"), ("y", "y", "x", "x"), ("x", "y", "y", "x"), ("x", "x", "y", "x"))
+CORNER = (("x", "x", "x", "y"), ("y", "x", "y", "x"), ("x", "x", "y", "y"), ("x", "x", "y", "x"))
 OUTER = (False, False, True, True)
 ORDER = (
-    (OWN, 0, 0), (OWN, 1, 0), (NORM, 7, 0), (OWN, 3, 0), (OWN, 2, 0), (NORM, 2, 0),
-    (HOP, 0, 1), (NORM, 5, 0), (HOP, 1, 1), (HOP, 0, 2), (EDGE, 1, 0), (HOP, 0, 3),
-    (HOP, 1, 2), (NORM, 0, 0), (HOP, 1, 3), (GROUP, 3, 1), (NORM, 4, 0), (HOP, 2, 1),
-    (GROUP, 1, 1), (GROUP, 0, 1), (PLACE, 0, 2), (PLACE, 0, 1), (NORM, 3, 0), (EDGE, 0, 0),
-    (GROUP, 0, 2), (HOP, 3, 1), (HOP, 2, 2), (PLACE, 1, 1), (PLACE, 0, 3), (NORM, 6, 0),
-    (HOP, 2, 3), (PLACE, 2, 0), (PLACE, 1, 2), (NORM, 1, 0), (PLACE, 1, 3), (PLACE, 1, 0),
-    (TIMES, 1, 0), (PLACE, 3, 0), (EDGE, 0, 2), (TIMES, 0, 2), (EDGE, 0, 1), (GROUP, 1, 3),
-    (GROUP, 2, 1), (TIMES, 0, 1), (HOP, 3, 2), (GROUP, 0, 3), (PLACE, 0, 0), (TIMES, 0, 0),
-    (GROUP, 2, 2), (EDGE, 1, 1), (HOP, 3, 3), (PLACE, 2, 1), (EDGE, 0, 3), (TIMES, 0, 3),
-    (TRADE, 0, 0), (EDGE, 1, 2), (EDGE, 2, 1), (TIMES, 1, 1), (GROUP, 2, 3), (EDGE, 1, 3),
-    (EDGE, 2, 0), (GROUP, 1, 2), (PLACE, 2, 3), (PLACE, 3, 2), (PLACE, 3, 1), (TIMES, 1, 3),
-    (EDGE, 2, 2), (EDGE, 3, 0), (PLACE, 2, 2), (TIMES, 1, 2), (TRADE, 1, 0), (TIMES, 3, 0),
-    (GROUP, 3, 2), (TIMES, 2, 1), (PLACE, 3, 3), (TIMES, 2, 2), (GROUP, 3, 3), (EDGE, 2, 3),
-    (TIMES, 2, 0), (TIMES, 2, 3), (TRADE, 2, 0), (EDGE, 3, 1), (TIMES, 3, 1), (EDGE, 3, 3),
-    (TIMES, 3, 3), (EDGE, 3, 2), (TIMES, 3, 2), (TRADE, 3, 0),
+    (OWN, 0, 0), (OWN, 1, 0), (NORM, 2, 0), (OWN, 3, 0), (OWN, 2, 0), (NORM, 7, 0),
+    (HOP, 0, 1), (HOP, 1, 1), (PLACE, 0, 0), (PLACE, 1, 0), (HOP, 0, 2), (NORM, 6, 0),
+    (HOP, 2, 2), (HOP, 1, 2), (HOP, 0, 3), (PLACE, 0, 1), (HOP, 2, 1), (NORM, 0, 0),
+    (PLACE, 1, 1), (HOP, 3, 1), (HOP, 1, 3), (EDGE, 1, 0), (GROUP, 1, 1), (PLACE, 0, 2),
+    (HOP, 3, 2), (PLACE, 2, 2), (NORM, 4, 0), (GROUP, 2, 1), (NORM, 3, 0), (GROUP, 0, 1),
+    (GROUP, 0, 3), (HOP, 3, 3), (NORM, 1, 0), (NORM, 5, 0), (HOP, 2, 3), (EDGE, 0, 1),
+    (PLACE, 1, 3), (EDGE, 1, 1), (TIMES, 1, 1), (GROUP, 0, 2), (GROUP, 1, 2), (TIMES, 0, 1),
+    (PLACE, 3, 2), (PLACE, 2, 0), (EDGE, 0, 0), (TIMES, 0, 0), (PLACE, 1, 2), (PLACE, 2, 1),
+    (PLACE, 0, 3), (GROUP, 3, 1), (GROUP, 2, 2), (EDGE, 0, 2), (TIMES, 0, 2), (GROUP, 1, 3),
+    (EDGE, 0, 3), (PLACE, 3, 0), (TIMES, 0, 3), (TRADE, 0, 0), (TIMES, 1, 0), (GROUP, 2, 3),
+    (PLACE, 3, 1), (PLACE, 2, 3), (EDGE, 1, 3), (TIMES, 1, 3), (PLACE, 3, 3), (EDGE, 1, 2),
+    (TIMES, 1, 2), (EDGE, 2, 2), (EDGE, 2, 0), (TIMES, 2, 0), (TRADE, 1, 0), (EDGE, 2, 1),
+    (TIMES, 2, 1), (EDGE, 3, 0), (TIMES, 3, 0), (GROUP, 3, 2), (EDGE, 3, 1), (TIMES, 2, 2),
+    (EDGE, 2, 3), (TIMES, 2, 3), (TRADE, 2, 0), (TIMES, 3, 1), (EDGE, 3, 2), (TIMES, 3, 2),
+    (GROUP, 3, 3), (EDGE, 3, 3), (TIMES, 3, 3), (TRADE, 3, 0),
 )
 MESH = pl.DeviceIdType.MESH
 
@@ -75,7 +75,7 @@
     grid, head_size,
     tokens, gain_in, w_key, w_value, queries_in, head_shift_in, key_shift_in,
     cache, read,
-    raw, normed, weights, acc, outgoing, incoming, totals, parts,
+    raw, normed, weights, acc, outgoing, incoming, parts,
     gain, queries, head_shift, key_shift,
     send_sem, piece_sem, cross_sem, last_sem, load_sem,
 ):
@@ -88,6 +88,7 @@
     blocks, _, span = weights.shape
     leads = sections if sections > 2 else 1
     leading = section == sections - 1
+    merged = 2 if leads == 1 else 1
     piece = shard // (groups * leads)
     kv_heads, heads = head_shift.shape
     seqs = seats // kv_heads
@@ -179,19 +180,19 @@
     def to_places(m, r, g):
         block, sem = piece_at(m, r, 0, g)
         for j in range(1, inner):
-            push(block, block, send_sem.at[m], sem, sp=lane * inner + lax.rem(place + j, inner))
+            push(block, block, send_sem.at[m // merged], sem, sp=lane * inner + lax.rem(place + j, inner))
             sent[m] += 1
 
     def to_groups(m, r, j):
         block, sem = piece_at(m, r, j, 0)
         for g in range(1, groups):
-            push(block, block, send_sem.at[m], sem, gr=lax.rem(group + g, groups))
+            push(block, block, send_sem.at[m // merged], sem, gr=lax.rem(group + g, groups))
             sent[m] += 1
 
     def to_sections(m, r, j, g):
         block, _ = piece_at(m, r, j, g)
         for t in range(1, sections):
-            push(block, block, send_sem.at[m], cross_sem.at[m, r], tp=lax.rem(section + t, sections))
+            push(block, block, send_sem.at[m // merged], cross_sem.at[m, r], tp=lax.rem(section + t, sections))
             sent[m] += 1
 
     def outer(m):
@@ -209,17 +210,17 @@
 
         @pl.when(lane > 0)
         def _():
-            push(block, block, send_sem.at[blocks + m], sem, sp=seat - inner)
+            push(block, block, send_sem.at[m // merged], sem, sp=seat - inner)
 
         @pl.when(lane < depth - 1)
         def _():
-            push(block, block, send_sem.at[blocks + m], sem, sp=seat + inner)
+            push(block, block, send_sem.at[m // merged], sem, sp=seat + inner)
 
         if outer(m):
             for g in range(1, groups):
                 other, its_sem = piece_at(m, 0, 0, g)
                 across = lane + 1 - 2 * lax.rem(lane, 2)
-                push(other, other, send_sem.at[blocks + m], its_sem, sp=across * inner + place)
+                push(other, other, send_sem.at[m // merged], its_sem, sp=across * inner + place)
         to_places(m, 0, 0)
         if CORNER[m % len(CORNER)][0] == "y":
             for g in range(1, groups):
@@ -233,7 +234,7 @@
 
         @pl.when((onward >= 0) & (onward < depth))
         def _():
-            push(block, block, send_sem.at[blocks + m], sem, sp=onward * inner + place)
+            push(block, block, send_sem.at[m // merged], sem, sp=onward * inner + place)
 
         to_places(m, r, 0)
         if not (outer(m) and r == 1):
@@ -307,41 +308,38 @@
         both = jnp.concatenate([weights[2 * k, pl.ds(start, long), :], weights[2 * k + 1, pl.ds(start, long), :]], axis=1)
         out = jnp.dot(normed[:, pl.ds(start, long)], both, preferred_element_type=jnp.float32)
         for m in range(2):
-            add(2 * k + m, out[:, m * span:(m + 1) * span])
+            add(2 * k + m, out[:, m * span:(m + 1) * span].T)
 
     def step_times(m, r):
         crossed(m, r)
         long = inner * shard
         start = pl.multiple_of(ranks[r] * long, long)
-        out = jnp.dot(normed[:, pl.ds(start, long)], weights[m, pl.ds(start, long), :], preferred_element_type=jnp.float32)
-        add(m, out)
+        add(m, lax.dot_general(
+            weights[m, pl.ds(start, long), :], normed[:, pl.ds(start, long)], (((0,), (1,)), ((), ())),
+            preferred_element_type=jnp.float32,
+        ))
 
     def step_trade(m, _):
         kind, part = m // per_kind, m % per_kind
+        block = acc[m].T
         for seq in range(seqs):
             for i in range(per_block):
                 cut = slice(i * head_size, (i + 1) * head_size)
-                first = acc[m, seq * sub:seq * sub + half, cut]
-                second = acc[m, seq * sub + half:(seq + 1) * sub, cut]
+                first = block[seq * sub:seq * sub + half, cut]
+                second = block[seq * sub + half:(seq + 1) * sub, cut]
                 outgoing[m, seq * per_block + i] = jnp.concatenate([first, second], axis=1).astype(jnp.bfloat16)
-        home = seat // kv_heads
-        for s in range(seqs):
-            seq = lax.rem(home + 1 + s, seqs)
+        for seq in range(seqs):
             for i in range(per_block):
                 to = seq * kv_heads + part * per_block + i
                 at = seq * per_block + i
 
-                def send():
+                @pl.when(seat != to)
+                def _():
                     push(outgoing.at[m, at], incoming.at[kind, seat], last_sem.at[kind], last_sem.at[2 + kind], sp=to)
 
-                if s < seqs - 1:
-                    send()
-                else:
-                    pl.when(to != seat)(send)
-
-                    @pl.when(to == seat)
-                    def _():
-                        incoming[kind, pl.ds(seat, 1)] = outgoing[m, pl.ds(at, 1)]
+                @pl.when(seat == to)
+                def _():
+                    incoming[kind, to] = outgoing[m, at]
 
     pl.semaphore_wait(barrier, inner + groups + sections - 3 + (lane + depth - 1) // depth + (2 * depth - 2 - lane) // depth)
     calls = (step_norm, step_own, step_lane, step_group, step_place, step_corner, step_times, step_pair, step_trade)
@@ -394,30 +392,17 @@
     local = jnp.concatenate(
         [jnp.concatenate(local[0::2], axis=1), jnp.concatenate(local[1::2], axis=1)], axis=0
     ).astype(jnp.bfloat16)
-    totals[section] = jnp.broadcast_to(running, totals.shape[1:])
-    for t in range(1, sections):
-        push(totals.at[section], totals.at[section], last_sem.at[4], last_sem.at[5], tp=lax.rem(section + t, sections))
     trace.__exit__(None, None, None)
-    trace = jax.named_scope("totals_in")
-    trace.__enter__()
-    if sections > 1:
-        settle(totals.at[pl.ds(0, sections - 1)], last_sem.at[5])
-    carry = jnp.zeros((heads, head_size), jnp.float32)
-    for t in reversed(range(sections)):
-        carry = carry + jnp.where(section < t, totals[t][:, :head_size], 0.0)
-    carry = jnp.exp(carry)
-    trace.__exit__(None, None, None)
-
     with jax.named_scope("values_in"):
         settle(incoming.at[1, pl.ds(0, seats - 1)], last_sem.at[3])
     trace = jax.named_scope("part")
     trace.__enter__()
     values = incoming[1].reshape(seats * half, 2 * head_size)
     part = jnp.dot(local, values, preferred_element_type=jnp.float32)
-    part = carry * (part[:heads, :head_size] + part[heads:, head_size:])
-    parts[section] = jnp.concatenate([part, part], axis=1)
+    part = part[:heads, :head_size] + part[heads:, head_size:]
+    parts[section] = jnp.concatenate([part, jnp.broadcast_to(running, part.shape)], axis=1)
     for t in range(1, sections):
-        push(parts.at[section], parts.at[section], last_sem.at[6], last_sem.at[7], tp=lax.rem(section + t, sections))
+        push(parts.at[section], parts.at[section], last_sem.at[4], last_sem.at[5], tp=lax.rem(section + t, sections))
     trace.__exit__(None, None, None)
     trace = jax.named_scope("cache")
     trace.__enter__()
@@ -427,12 +412,11 @@
             start = (2 * q + h) * half
             cache[0, start:start + half, :] = jnp.concatenate([incoming[0, q][:, cut], incoming[1, q][:, cut]], axis=1)
     def drain():
-        for m in range(blocks):
-            settle_pieces(sent[m], send_sem.at[m])
+        for pair in range(blocks // merged):
+            both = range(merged * pair, merged * (pair + 1))
             for k in range(depth):
-                count = (k + 1 if k < depth - 1 else 0) + (depth - k if k > 0 else 0) + (groups - 1) * outer(m)
-                if count:
-                    pl.when(lane == k)(lambda count=count: settle_pieces(count, send_sem.at[blocks + m]))
+                count = sum(sent[m] + (k + 1) * (k < depth - 1) + (depth - k) * (k > 0) + (groups - 1) * outer(m) for m in both)
+                pl.when(lane == k)(lambda count=count: settle_pieces(count, send_sem.at[pair]))
 
     lead(drain)
     for kind in range(2):
@@ -441,14 +425,15 @@
     trace = jax.named_scope("parts_in")
     trace.__enter__()
     if sections > 1:
-        settle(totals.at[pl.ds(0, sections - 1)], last_sem.at[4])
-        settle(parts.at[pl.ds(0, sections - 1)], last_sem.at[6])
-        settle(parts.at[pl.ds(0, sections - 1)], last_sem.at[7])
-    total = parts[0]
-    for t in range(1, sections):
-        total = total + parts[t]
+        settle(parts.at[pl.ds(0, sections - 1)], last_sem.at[4])
+        settle(parts.at[pl.ds(0, sections - 1)], last_sem.at[5])
+    total = jnp.zeros((heads, head_size), jnp.float32)
+    carry = jnp.zeros((heads, head_size), jnp.float32)
+    for t in reversed(range(sections)):
+        total = total + jnp.exp(carry) * parts[t][:, :head_size]
+        carry = carry + parts[t][:, head_size:]
     for g in range(heads):
-        read[:, g * head_size:(g + 1) * head_size] = total[g:g + 1, :head_size]
+        read[:, g * head_size:(g + 1) * head_size] = total[g:g + 1, :]
     trace.__exit__(None, None, None)
 
 
@@ -485,19 +470,18 @@
             pltpu.VMEM((rows, width), jnp.bfloat16),
             pltpu.VMEM((rows, width), jnp.bfloat16),
             pltpu.VMEM((blocks, width, LANES), jnp.bfloat16),
-            pltpu.VMEM((blocks, rows, LANES), jnp.float32),
+            pltpu.VMEM((blocks, LANES, rows), jnp.float32),
             pltpu.VMEM((blocks, seqs * LANES // head_size, sub // 2, 2 * head_size), jnp.bfloat16),
             pltpu.VMEM((2, seats, sub // 2, 2 * head_size), jnp.bfloat16),
-            pltpu.VMEM((sections, heads, 2 * head_size), jnp.float32),
             pltpu.VMEM((sections, heads, 2 * head_size), jnp.float32),
             pltpu.VMEM(ln_gain.shape, ln_gain.dtype),
             pltpu.VMEM(queries.shape, queries.dtype),
             pltpu.VMEM(head_shift.shape, head_shift.dtype),
             pltpu.VMEM(key_shift.shape, key_shift.dtype),
-            pltpu.SemaphoreType.DMA((2 * blocks,)),
+            pltpu.SemaphoreType.DMA((blocks,)),
             pltpu.SemaphoreType.DMA((blocks, seats, groups)),
             pltpu.SemaphoreType.DMA((blocks, depth)),
-            pltpu.SemaphoreType.DMA((8,)),
+            pltpu.SemaphoreType.DMA((6,)),
             pltpu.SemaphoreType.DMA((blocks + FILLS + 4,)),
         ],
         compiler_params=pltpu.CompilerParams(

time: 37.1 us -> 35.2 us (0.949)
  Pallas kernels: 36.3 us -> 34.4 us
    pallas_call x1, Pallas kernels: 35.5 us -> 33.6 us  [local(): pl.pallas_call(functools.partial(body, grid, head_size), out_shape=(jax.S...]
where the time goes in v4:
time: 35.2 us; the launch traced here: 35.1 us
  Pallas kernels  34.4 us (98%)
  between operations  0.64 us (2%)
    pallas_call x1, Pallas kernels, local(): pl.pallas_call(functools.partial(body, grid, head_size), out_shape=(jax.S...  33.6 us
    pallas_call x1, Pallas kernels, local(): pl.pallas_call(hand_over, out_shape=(jax.ShapeDtypeStruct(cache.shape, ca...  0.81 us

profile of v4, /device:TPU:13, one launch (start us, length us, event | category | flops | bytes accessed | tf_op | source)
XLA Modules:
  0.0 35.1 jit_solution(6884318586150255748)
XLA Ops:
  0.6 33.6 %shard_map.86 = (bf16[1,2048,128]{2,1,0:T(8,128)(2,1)S(1)}, f32[1,512]{1,0:T(1,128)S(1)}) custom-call(bf16[512,4096]{1,0:T(8,128)(2,1)} %bitcast.1, bf16[4096]{0:T(1024)(128)(2,1)} %gain_in.1, bf16[512,256]{1,0:T(8,128)(2,1)} %w_key.1, bf16[512,256]{1,0:T(8,128)(2,1)} %w_value.1, bf16[1,512]{1,0:T(2,128)(2,1)} %queries_in.1, f32[4,8]{1,0:T(4,128)} %head_shift_in.1, ...), custom_call_target="tpu_custom_call" | custom-call | tf_op jit(solution)/shard_map/pallas_call | solution.py:461
  34.2 0.8 %shard_map.87 = (bf16[1,2048,128]{2,1,0:T(8,128)(2,1)}, f32[1,512]{1,0:T(1,128)}) custom-call(bf16[1,2048,128]{2,1,0:T(8,128)(2,1)S(1)} %get-tuple-element.4.cache, f32[1,512]{1,0:T(1,128)S(1)} %get-tuple-element.5.read), custom_call_target="tpu_custom_call" | custom-call | tf_op jit(solution)/shard_map/pallas_call | solution.py:491

commit v5 on v4

--- a/solution.py
+++ b/solution.py
@@ -10,7 +10,7 @@
 epsilon = 1e-05
 LANES = 128
 NORM, OWN, HOP, GROUP, PLACE, EDGE, TIMES, PAIR, TRADE = range(9)
-FILLS = 4
+FILLS = 1
 NORMS = 8
 BASES = (0.0, 2.0, 4.0, 6.0)
 LANE_STEP, GROUP_AT, PLACE_AT, CORNER_AT, TIMES_AT, OWN_AT = 1.5, 3.0, 2.0, 5.0, 7.0, -3.0
@@ -335,7 +335,7 @@
 
                 @pl.when(seat != to)
                 def _():
-                    push(outgoing.at[m, at], incoming.at[kind, seat], last_sem.at[kind], last_sem.at[2 + kind], sp=to)
+                    push(outgoing.at[m, at], incoming.at[kind, seat], last_sem.at[0], last_sem.at[1 + kind], sp=to)
 
                 @pl.when(seat == to)
                 def _():
@@ -367,7 +367,7 @@
     ).astype(jnp.float32)
 
     with jax.named_scope("keys_in"):
-        settle(incoming.at[0, pl.ds(0, seats - 1)], last_sem.at[2])
+        settle(incoming.at[0, pl.ds(0, seats - 1)], last_sem.at[1])
     trace = jax.named_scope("logits")
     trace.__enter__()
     keys = incoming[0].reshape(seats * half, 2 * head_size)
@@ -394,7 +394,7 @@
     ).astype(jnp.bfloat16)
     trace.__exit__(None, None, None)
     with jax.named_scope("values_in"):
-        settle(incoming.at[1, pl.ds(0, seats - 1)], last_sem.at[3])
+        settle(incoming.at[1, pl.ds(0, seats - 1)], last_sem.at[2])
     trace = jax.named_scope("part")
     trace.__enter__()
     values = incoming[1].reshape(seats * half, 2 * head_size)
@@ -402,7 +402,7 @@
     part = part[:heads, :head_size] + part[heads:, head_size:]
     parts[section] = jnp.concatenate([part, jnp.broadcast_to(running, part.shape)], axis=1)
     for t in range(1, sections):
-        push(parts.at[section], parts.at[section], last_sem.at[4], last_sem.at[5], tp=lax.rem(section + t, sections))
+        push(parts.at[section], parts.at[section], last_sem.at[3], last_sem.at[4], tp=lax.rem(section + t, sections))
     trace.__exit__(None, None, None)
     trace = jax.named_scope("cache")
     trace.__enter__()
@@ -419,14 +419,13 @@
                 pl.when(lane == k)(lambda count=count: settle_pieces(count, send_sem.at[pair]))
 
     lead(drain)
-    for kind in range(2):
-        settle(incoming.at[kind, pl.ds(0, seats - 1)], last_sem.at[kind])
+    settle(incoming.at[:, pl.ds(0, seats - 1)], last_sem.at[0])
     trace.__exit__(None, None, None)
     trace = jax.named_scope("parts_in")
     trace.__enter__()
     if sections > 1:
+        settle(parts.at[pl.ds(0, sections - 1)], last_sem.at[3])
         settle(parts.at[pl.ds(0, sections - 1)], last_sem.at[4])
-        settle(parts.at[pl.ds(0, sections - 1)], last_sem.at[5])
     total = jnp.zeros((heads, head_size), jnp.float32)
     carry = jnp.zeros((heads, head_size), jnp.float32)
     for t in reversed(range(sections)):
@@ -478,10 +477,10 @@
             pltpu.VMEM(queries.shape, queries.dtype),
             pltpu.VMEM(head_shift.shape, head_shift.dtype),
             pltpu.VMEM(key_shift.shape, key_shift.dtype),
-            pltpu.SemaphoreType.DMA((blocks,)),
+            pltpu.SemaphoreType.DMA((blocks if sections > 2 else blocks // 2,)),
             pltpu.SemaphoreType.DMA((blocks, seats, groups)),
             pltpu.SemaphoreType.DMA((blocks, depth)),
-            pltpu.SemaphoreType.DMA((6,)),
+            pltpu.SemaphoreType.DMA((5,)),
             pltpu.SemaphoreType.DMA((blocks + FILLS + 4,)),
         ],
         compiler_params=pltpu.CompilerParams(

time: 35.2 us -> 35.5 us (level)
  no operation moved by 1% of the time
where the time goes in v5:
time: 35.5 us; the launch traced here: 35.2 us
  Pallas kernels  34.6 us (97%)
  between operations  0.64 us (2%)
    pallas_call x1, Pallas kernels, local(): pl.pallas_call(functools.partial(body, grid, head_size), out_shape=(jax.S...  33.8 us
    pallas_call x1, Pallas kernels, local(): pl.pallas_call(hand_over, out_shape=(jax.ShapeDtypeStruct(cache.shape, ca...  0.81 us

profile of v5, /device:TPU:13, one launch (start us, length us, event | category | flops | bytes accessed | tf_op | source)
XLA Modules:
  0.0 35.2 jit_solution(4177214491782001913)
XLA Ops:
  0.6 33.8 %shard_map.86 = (bf16[1,2048,128]{2,1,0:T(8,128)(2,1)S(1)}, f32[1,512]{1,0:T(1,128)S(1)}) custom-call(bf16[512,4096]{1,0:T(8,128)(2,1)} %bitcast.1, bf16[4096]{0:T(1024)(128)(2,1)} %gain_in.1, bf16[512,256]{1,0:T(8,128)(2,1)} %w_key.1, bf16[512,256]{1,0:T(8,128)(2,1)} %w_value.1, bf16[1,512]{1,0:T(2,128)(2,1)} %queries_in.1, f32[4,8]{1,0:T(4,128)} %head_shift_in.1, ...), custom_call_target="tpu_custom_call" | custom-call | tf_op jit(solution)/shard_map/pallas_call | solution.py:460
  34.4 0.8 %shard_map.87 = (bf16[1,2048,128]{2,1,0:T(8,128)(2,1)}, f32[1,512]{1,0:T(1,128)}) custom-call(bf16[1,2048,128]{2,1,0:T(8,128)(2,1)S(1)} %get-tuple-element.4.cache, f32[1,512]{1,0:T(1,128)S(1)} %get-tuple-element.5.read), custom_call_target="tpu_custom_call" | custom-call | tf_op jit(solution)/shard_map/pallas_call | solution.py:490
